TPU v7x, 128 devices: a whole 4x4x4 slice. The times are simulated.
128 devices in a mesh: rep: 2 (over z_hi), fs: 32 (over z_lo, y, x), tp: 2 (over core).
Axes of the slice: x: 4, y: 4, z: 4 (z_hi: 2, z_lo: 2; z = z_hi * 2 + z_lo), core: 2. Of those that a mesh axis runs over, the one named last changes fastest.
Arguments:
- tokens: bfloat16 [65536, 2048], P(('rep', 'fs', 'tp')), parts along dimension 0, may hold values from -6 to 6
- mix_gain: float32 [2048], replicated, may hold values from 0.1 to 1.9
- w_query: bfloat16 [2048, 512], P('fs', 'tp'), may hold values from -0.125 to 0.125
- w_key: bfloat16 [2048, 512], P('fs', 'tp'), may hold values from -0.125 to 0.125
- w_value: bfloat16 [2048, 1024], P('fs', 'tp'), may hold values from -0.125 to 0.125
- w_out: bfloat16 [1024, 2048], P('tp', 'fs'), may hold values from -0.1875 to 0.1875
- ffn_gain: float32 [2048], replicated, may hold values from 0.1 to 1.9
- w_ffgate: bfloat16 [2048, 2816], P('fs', 'tp'), may hold values from -0.125 to 0.125
- w_ffup: bfloat16 [2048, 2816], P('fs', 'tp'), may hold values from -0.125 to 0.125
- conv_gate: float32 [3, 2816], replicated, may hold values from -3 to 3
- conv_up: float32 [3, 2816], replicated, may hold values from -3 to 3
- w_down: bfloat16 [2816, 2048], P('tp', 'fs'), may hold values from -0.109375 to 0.109375
Outputs:
- layer_out: bfloat16 [65536, 2048], P(('rep', 'fs', 'tp')), parts along dimension 0
There are 2 independent parts, one for each index of `rep`. A program takes and returns all parts, laid end to end along the dimension named above; an argument that names none is the same for every part. Nothing has to cross between parts.
All inputs are finite; a program needn't handle non-finite values.
Results may differ from a plain program's by a relative error of at most 0.014.
Values may be sent and summed in bfloat16 or wider, within the bound.
A program may use at most 128 MiB of HBM per device.

v0:
```python
import jax
import jax.numpy as jnp
from jax import lax
from jax.sharding import PartitionSpec as P

HEADS = 4
DK = 128
DV = 256
KERNEL = 3
BLOCK = 128
LENGTH = 1024


epsilon = 1e-06


def in_one_piece(arrays, axis, dim, along):
    both = jnp.concatenate(arrays, axis=along)
    out, at, done = (lax.all_gather(both, axis, axis=dim, tiled=True), 0, [])
    for a in arrays:
        done.append(lax.slice_in_dim(out, at, at + a.shape[along], axis=along))
        at += a.shape[along]
    return tuple(done)


def copy_for_each(shard, axis):
    length = lax.axis_size(axis)
    return lax.all_to_all(
        jnp.broadcast_to(shard[None], (length, *shard.shape)), axis, 0, 0, tiled=True
    )


def in_order(pieces, dim):
    pieces = jnp.moveaxis(pieces, 0, dim)
    dims = pieces.shape
    return pieces.reshape(*dims[:dim], dims[dim] * dims[dim + 1], *dims[dim + 2 :])


def collect(shard, axis, dim):
    pieces = copy_for_each(shard, axis)
    return in_order(pieces, dim)


def in_blocks(shard, dim, length):
    dims = shard.shape
    pieces = shard.reshape(*dims[:dim], length, dims[dim] // length, *dims[dim + 1 :])
    return jnp.moveaxis(pieces, dim, 0)


def sent_and_summed(shard, axis, dim):
    length = lax.axis_size(axis)
    pieces = lax.all_to_all(in_blocks(shard, dim, length), axis, 0, 0, tiled=True)
    return jnp.sum(pieces.astype(jnp.float32), axis=0)


def rms_rows(matrix, scale_vec):
    values = matrix.astype(jnp.float32)
    factor = lax.rsqrt(jnp.mean(values * values, axis=-1, keepdims=True) + epsilon)
    return (values * factor * scale_vec).astype(jnp.bfloat16)


def rotate_heads(matrix):
    length = matrix.shape[0]
    half_width = matrix.shape[-1] // 2
    inverse = 10000.0 ** (-jnp.arange(half_width, dtype=jnp.float32) * 2.0 / (2 * half_width))
    angles = jnp.arange(length, dtype=jnp.float32)[:, None] * inverse[None, :]
    cosine = jnp.cos(angles)[:, None, :]
    sine = jnp.sin(angles)[:, None, :]
    values = matrix.astype(jnp.float32)
    first_half = values[..., :half_width]
    second_half = values[..., half_width:]
    return jnp.concatenate(
        [first_half * cosine - second_half * sine, first_half * sine + second_half * cosine],
        axis=-1,
    )


def retain_blocks(rot_query, rot_key, value, rates, block_len):
    length, head_count, width_k = rot_query.shape
    width_v = value.shape[-1]
    blocks = length // block_len
    query4 = rot_query.reshape(blocks, block_len, head_count, width_k)
    key4 = rot_key.reshape(blocks, block_len, head_count, width_k)
    value4 = value.reshape(blocks, block_len, head_count, width_v)
    places = jnp.arange(block_len, dtype=jnp.float32)
    spacing = places[:, None] - places[None, :]
    inside = jnp.where(
        spacing[None] >= 0, jnp.exp(-jnp.maximum(spacing, 0.0)[None] * rates[:, None, None]), 0.0
    )
    scores = jnp.einsum("cihd,cjhd->chij", query4, key4, preferred_element_type=jnp.float32)
    weights = (scores * inside[None]).astype(jnp.bfloat16)
    inner_part = jnp.einsum("chij,cjhe->cihe", weights, value4, preferred_element_type=jnp.float32)
    tail_decay = jnp.exp(-(block_len - 1.0 - places)[:, None] * rates[None, :])
    decayed = (key4.astype(jnp.float32) * tail_decay[None, :, :, None]).astype(jnp.bfloat16)
    states = jnp.einsum("cjhd,cjhe->chde", decayed, value4, preferred_element_type=jnp.float32)
    passing = jnp.exp(-block_len * rates)[:, None, None]

    def advance(carried, fresh):
        return (carried * passing + fresh, carried)

    _, before = lax.scan(advance, jnp.zeros((head_count, width_k, width_v), jnp.float32), states)
    onset_decay = jnp.exp(-(places + 1.0)[:, None] * rates[None, :])
    cross_part = (
        jnp.einsum("cihd,chde->cihe", query4.astype(jnp.float32), before)
        * onset_decay[None, :, :, None]
    )
    return (inner_part + cross_part).reshape(length, head_count, width_v)


def head_norm(retained):
    average = jnp.mean(retained, axis=-1, keepdims=True)
    centered = retained - average
    return centered * lax.rsqrt(jnp.mean(centered * centered, axis=-1, keepdims=True) + epsilon)


def causal_taps(matrix, kernel_w):
    length = matrix.shape[0]
    padded = jnp.pad(matrix.astype(jnp.float32), ((KERNEL - 1, 0), (0, 0)))
    total = jnp.zeros((length, matrix.shape[1]), jnp.float32)
    for tap_idx in range(KERNEL):
        total = total + kernel_w[tap_idx][None, :] * padded[tap_idx : tap_idx + length]
    return total


def collect_ffn(w_ffgate, w_ffup):
    return in_one_piece((w_ffgate, w_ffup), "fs", 0, 1)


def body(
    tokens,
    mix_gain,
    w_query,
    w_key,
    w_value,
    w_out,
    ffn_gain,
    w_ffgate,
    w_ffup,
    conv_gate,
    conv_up,
    w_down,
):
    tp_rank = lax.axis_index("tp")
    heads_here = w_query.shape[1] // DK
    ffn_pair = None
    normed = rms_rows(tokens, mix_gain)
    query_w, key_w, value_w = in_one_piece((w_query, w_key, w_value), "fs", 0, 1)
    qk_cols = query_w.shape[1]
    pieces = lax.all_gather(normed, "tp", axis=0, tiled=True)
    joined = jnp.concatenate(
        [
            jnp.dot(pieces, query_w, preferred_element_type=jnp.float32),
            jnp.dot(pieces, key_w, preferred_element_type=jnp.float32),
            jnp.dot(pieces, value_w, preferred_element_type=jnp.float32),
        ],
        axis=1,
    ).astype(jnp.bfloat16)
    length = joined.shape[0]
    query = joined[:, :qk_cols].reshape(length, heads_here, DK)
    key = joined[:, qk_cols : 2 * qk_cols].reshape(length, heads_here, DK)
    value = joined[:, 2 * qk_cols :].reshape(length, heads_here, DV)
    rot_query = rotate_heads(query).astype(jnp.bfloat16)
    rot_key = (rotate_heads(key) * DK ** (-0.5)).astype(jnp.bfloat16)
    head_ids = (tp_rank * heads_here + jnp.arange(heads_here, dtype=jnp.int32)).astype(jnp.float32)
    rates = 1.0 / 16.0 * (32.0 / LENGTH) ** (head_ids / (HEADS - 1))
    retained = retain_blocks(rot_query, rot_key, value, rates, BLOCK)
    hidden = head_norm(retained).reshape(length, heads_here * DV).astype(jnp.bfloat16)
    out_full = collect(w_out, "fs", 1)
    mix_sum = sent_and_summed(
        jnp.dot(hidden, out_full, preferred_element_type=jnp.float32).astype(jnp.bfloat16), "tp", 0
    )
    resid = (tokens.astype(jnp.float32) + mix_sum).astype(jnp.bfloat16)
    normed_ffn = rms_rows(resid, ffn_gain)
    ff_here = w_ffgate.shape[1]
    ffn_pair = collect_ffn(w_ffgate, w_ffup)
    gate_w, up_w = ffn_pair
    pieces = lax.all_gather(normed_ffn, "tp", axis=0, tiled=True)
    both_pre = jnp.concatenate(
        [
            jnp.dot(pieces, gate_w, preferred_element_type=jnp.float32),
            jnp.dot(pieces, up_w, preferred_element_type=jnp.float32),
        ],
        axis=1,
    ).astype(jnp.bfloat16)
    gate_pre = both_pre[:, :ff_here]
    up_pre = both_pre[:, ff_here:]
    gate_taps = lax.dynamic_slice_in_dim(conv_gate, tp_rank * ff_here, ff_here, 1)
    up_taps = lax.dynamic_slice_in_dim(conv_up, tp_rank * ff_here, ff_here, 1)
    activ = (jax.nn.silu(causal_taps(gate_pre, gate_taps)) * causal_taps(up_pre, up_taps)).astype(
        jnp.bfloat16
    )
    down_full = lax.all_gather(w_down, "fs", axis=1, tiled=True)
    ffn_sum = sent_and_summed(
        jnp.dot(activ, down_full, preferred_element_type=jnp.float32).astype(jnp.bfloat16), "tp", 0
    )
    return (resid.astype(jnp.float32) + ffn_sum).astype(jnp.bfloat16)


def solution(mesh):
    placed = (
        P(("rep", "fs", "tp"), None),
        P(),
        P("fs", "tp"),
        P("fs", "tp"),
        P("fs", "tp"),
        P("tp", "fs"),
        P(),
        P("fs", "tp"),
        P("fs", "tp"),
        P(),
        P(),
        P("tp", "fs"),
    )
    return jax.shard_map(
        body, mesh=mesh, in_specs=placed, out_specs=P(("rep", "fs", "tp"), None), check_vma=False
    )
```

profile of v0, /device:TPU:1, one launch (start us, length us, event | category | flops | bytes accessed | tf_op | source)
XLA Modules:
  0.0 637.9 jit_solution(8390424234193751009)
XLA Ops:
  6.6 2.1 fusion.6
  8.7 3.5 fusion.8
  12.3 0.7 pad_maximum_fusion.2
  13.0 1.5 broadcast_in_dim.25
  14.5 9.3 %all-to-all-start = ((bf16[32,512,64]{1,2,0:T(8,128)(2,1)}), bf16[32,512,64]{1,2,0:T(8,128)(2,1)}, u32[]{:S(2)}, u32[]{:S(2)}) async-start(bf16[32,512,64]{1,2,0:T(8,128)(2,1)} %broadcast_in_dim.25), calls=%async_computation | async-start | bytes 4194304 | tf_op jit(solution)/shard_map/all_to_all | solution.py:28
  24.2 1.0 fusion.44
  25.2 7.1 %all-gather.6.cloned.1.call-done = bf16[1024,2048]{1,0:T(8,128)(2,1)} async-done(((bf16[512,2048]{1,0:T(8,128)(2,1)}), bf16[1024,2048]{1,0:T(8,128)(2,1)}) %all-gather.6.cloned.1.call-update) | async-done | bytes 4194320 | tf_op jit(solution)/shard_map/all_gather | solution.py:149
  32.3 140.7 %all-gather.8.cloned.1.call-done = bf16[2048,1024]{1,0:T(8,128)(2,1)} async-done(((bf16[64,1024]{1,0:T(8,128)(2,1)}), bf16[2048,1024]{1,0:T(8,128)(2,1)}) %all-gather.8.cloned.1.call-update) | async-done | bytes 4194320 | tf_op jit(solution)/shard_map/all_gather | solution.py:19
  173.0 3.9 convolution_convert_fusion.3
  177.1 2.5 convolution_convert_fusion.2
  179.7 1.1 subtract_convert_fusion
  181.8 6.2 fusion.31
  187.9 1.3 reshape_reshape.3
  189.6 0.8 copy-done.1
  190.4 0.6 fusion.38
  191.0 6.5 %while.13 = (s32[]{:T(128)}, f32[2,128,256]{2,1,0:T(8,128)S(1)}, bf16[8,2,128,256]{3,2,1,0:T(8,128)(2,1)}, f32[8,2,128,256]{3,2,1,0:T(8,128)S(1)}, s32[]{:T(128)}, /*index=5*/s32[]{:T(128)}, s32[]{:T(128)}) while((s32[]{:T(128)}, f32[2,128,256]{2,1,0:T(8,128)S(1)}, bf16[8,2,128,256]{3,2,1,0:T(8,128)(2,1)}, ...), condition=%wide.region_2.3_spmd.clone, body=%wide.region_1.2_spmd.clone.sunk | while | flops 262155 | bytes 1180272 | solution.py:101
  191.0 0.7 bitcast_dynamic-update-slice_fusion.2
  191.8 0.7 bitcast_dynamic-update-slice_fusion.2
  192.6 0.7 bitcast_dynamic-update-slice_fusion.2
  193.4 0.7 bitcast_dynamic-update-slice_fusion.2
  194.3 0.7 bitcast_dynamic-update-slice_fusion.2
  195.1 0.7 bitcast_dynamic-update-slice_fusion.2
  195.9 0.7 bitcast_dynamic-update-slice_fusion.2
  196.7 0.7 bitcast_dynamic-update-slice_fusion.2
  197.5 1.0 copy.48
  198.8 1.2 copy.49
  200.3 3.2 fusion.45
  203.6 3.0 fusion.54
  206.8 0.7 multiply_reduce_fusion
  207.5 0.9 fusion.29
  208.3 0.5 copy.46
  208.9 4.0 convolution_convert_fusion.1
  212.9 27.5 %all_to_all.15 = bf16[2,512,2048]{2,1,0:T(8,128)(2,1)S(1)} all-to-all(bf16[2,512,2048]{2,1,0:T(8,128)(2,1)S(1)} %bitcast.73), channel_id=1, replica_groups=mesh['rep'=2,'fs'=32,'tp'=2] {'tp'}, dimensions={0} | all-to-all | bytes 8388608 | tf_op jit(solution)/shard_map/all_to_all | solution.py:52
  240.4 1.0 convert_reduce_fusion.1
  241.3 0.6 copy-done
  241.9 0.7 fusion.10
  242.7 1.9 fusion.12
  244.6 0.8 pad_maximum_fusion.1
  246.0 1.1 dynamic-slice_reduce_fusion.2
  247.1 15.1 %all-gather.10.cloned.1.call-done = bf16[1024,2048]{1,0:T(8,128)(2,1)} async-done(((bf16[512,2048]{1,0:T(8,128)(2,1)}), bf16[1024,2048]{1,0:T(8,128)(2,1)}) %all-gather.10.cloned.1.call-update) | async-done | bytes 4194320 | tf_op jit(solution)/shard_map/all_gather | solution.py:177
  262.2 155.1 %all-gather.12.cloned.1.call-done = bf16[2048,2816]{1,0:T(8,128)(2,1)} async-done(((bf16[64,2816]{1,0:T(8,128)(2,1)}), bf16[2048,2816]{1,0:T(8,128)(2,1)}) %all-gather.12.cloned.1.call-update) | async-done | bytes 11534352 | tf_op jit(solution)/shard_map/all_gather | solution.py:19
  417.3 11.8 %fusion.17 = f32[1024,1408]{1,0:T(8,128)} fusion(bf16[1024,2048]{1,0:T(8,128)(2,1)} %all-gather.10.cloned.1.call-done, bf16[2048,2816]{1,0:T(8,128)(2,1)} %all-gather.12.cloned.1.call-done), kind=kOutput, calls=%fused_computation.26 | convolution fusion | flops 5908463616 | bytes 15728640 | tf_op jit(solution)/shard_map/dot_general | solution.py:180
  429.1 8.5 %fusion.23 = f32[1024,1408]{1,0:T(8,128)} fusion(bf16[1024,2048]{1,0:T(8,128)(2,1)S(1)} %copy-done.13, bf16[2048,2816]{1,0:T(8,128)(2,1)S(1)} %copy-done.11), kind=kOutput, calls=%fused_computation.28 | convolution fusion | flops 5908463616 | bytes 15728640 | tf_op jit(solution)/shard_map/dot_general | solution.py:181
  437.6 139.5 %all-gather.14.cloned.1.call-done = bf16[1408,2048]{0,1:T(8,128)(2,1)} async-done(((bf16[1408,64]{0,1:T(8,128)(2,1)}), bf16[1408,2048]{0,1:T(8,128)(2,1)}) %all-gather.14.cloned.1.call-update) | async-done | bytes 5767184 | tf_op jit(solution)/shard_map/all_gather | solution.py:192
  577.1 23.0 %convolution_convert_fusion = bf16[1024,2048]{1,0:T(8,128)(2,1)} fusion(bf16[1408,2048]{0,1:T(8,128)(2,1)} %all-gather.14.cloned.1.call-done, f32[1024,1408]{1,0:T(8,128)} %fusion.23, f32[1024,1408]{1,0:T(8,128)} %fusion.17, f32[1408]{0:T(1024)S(1)} %get-tuple-element.59, f32[1408]{0:T(1024)S(1)} %get-tuple-element.58, f32[1408]{0:T(1024)S(1)} %get-tuple-element.57, ...), kind=kOutput, calls=%fused_computation.29 | convolution fusion | flops 5930745856 | bytes 21529600 | tf_op jit(solution)/shard_map/dot_general | solution.py:194
  600.1 28.2 %all_to_all.16 = bf16[2,512,2048]{2,1,0:T(8,128)(2,1)S(1)} all-to-all(bf16[2,512,2048]{2,1,0:T(8,128)(2,1)} %bitcast.72), channel_id=1, replica_groups=mesh['rep'=2,'fs'=32,'tp'=2] {'tp'}, dimensions={0} | all-to-all | bytes 8388608 | tf_op jit(solution)/shard_map/all_to_all | solution.py:52
  628.3 1.0 convert_reduce_fusion
  629.3 2.1 fusion.13
  (76 shorter events, 4.3 us)
Async XLA Ops:
  6.5 5.7 copy-start.7
  6.5 5.7 copy-start.8
  6.5 5.7 copy-start.9
  6.5 6.4 %copy-start.6 = (bf16[512,64]{0,1:T(8,128)(2,1)S(1)}, bf16[512,64]{0,1:T(8,128)(2,1)}, u32[]{:S(2)}) copy-start(bf16[512,64]{0,1:T(8,128)(2,1)} %param.19) | copy-start | bytes 196612
  6.5 25.8 %all-gather.6.cloned.1.call-start = ((), (), s32[]{:S(2)}) async-start(), calls=%async_computation.3 | async-start | bytes 6291456 | tf_op jit(solution)/shard_map/all_gather | solution.py:149
  12.2 160.8 %all-gather.8.cloned.1.call-start = ((), (), s32[]{:S(2)}) async-start(), calls=%async_computation.4 | async-start | bytes 4325376 | tf_op jit(solution)/shard_map/all_gather | solution.py:19
  14.5 194.4 %all-to-all-start = ((bf16[32,512,64]{1,2,0:T(8,128)(2,1)}), bf16[32,512,64]{1,2,0:T(8,128)(2,1)}, u32[]{:S(2)}, u32[]{:S(2)}) async-start(bf16[32,512,64]{1,2,0:T(8,128)(2,1)} %broadcast_in_dim.25), calls=%async_computation | async-start | bytes 4194304 | tf_op jit(solution)/shard_map/all_to_all | solution.py:28
  23.9 238.3 %all-gather.10.cloned.1.call-start = ((), (), s32[]{:S(2)}) async-start(), calls=%async_computation.5 | async-start | bytes 6291456 | tf_op jit(solution)/shard_map/all_gather | solution.py:177
  173.0 4.1 copy-start.12
  189.6 0.8 copy-start.1
  198.8 4.8 copy-start.2
  200.3 3.2 copy-start.3
  240.4 1.6 copy-start
  241.9 0.7 copy-start.10
  242.6 2.0 copy-start.4
  242.6 2.0 copy-start.5
  244.6 172.7 %all-gather.12.cloned.1.call-start = ((), (), s32[]{:S(2)}) async-start(), calls=%async_computation.6 | async-start | bytes 11894784 | tf_op jit(solution)/shard_map/all_gather | solution.py:19
  245.4 331.7 %all-gather.14.cloned.1.call-start = ((), (), s32[]{:S(2)}) async-start(), calls=%async_computation.7 | async-start | bytes 5947392 | tf_op jit(solution)/shard_map/all_gather | solution.py:192
  417.3 11.8 %copy-start.11 = (bf16[2048,2816]{1,0:T(8,128)(2,1)S(1)}, bf16[2048,2816]{1,0:T(8,128)(2,1)}, u32[]{:S(2)}) copy-start(bf16[2048,2816]{1,0:T(8,128)(2,1)} %all-gather.12.cloned.1.call-done) | copy-start | bytes 34603012
  417.3 11.9 %copy-start.13 = (bf16[1024,2048]{1,0:T(8,128)(2,1)S(1)}, bf16[1024,2048]{1,0:T(8,128)(2,1)}, u32[]{:S(2)}) copy-start(bf16[1024,2048]{1,0:T(8,128)(2,1)} %all-gather.10.cloned.1.call-done) | copy-start | bytes 12582916
Sparse Core Ops, SparseCore 0:
  12.3 19.9 all-gather.5
  34.0 138.9 all-gather.7
  244.7 17.4 all-gather.9
  263.7 153.5 all-gather.11
  418.8 158.2 all-gather.13
where the time goes:
time: 639 us; the launch traced here: 638 us
  waiting for transfers between devices  458 us (72%)
  matrix products  66.7 us (10%)
  blocking collectives  55.7 us (9%)
  other arithmetic  24.3 us (4%)
  between operations  13.5 us (2%)
  local copies, waits for them, and re-layouts  9.83 us (2%)
  starting transfers between devices  9.54 us (1%)
    all_gather x2, waiting for transfers between devices, in_one_piece(): out, at, done = (lax.all_gather(both, axis, axis=dim, tiled=True), 0, [])  296 us
    all_gather x1, waiting for transfers between devices, body(): down_full = lax.all_gather(w_down, 'fs', axis=1, tiled=True)  139 us
    all_to_all x2, blocking collectives, sent_and_summed(): lax.all_to_all(in_blocks(shard, dim, length), axis, 0, 0, tiled=True)  55.7 us
    dot_general x1, matrix products, body(): jnp.dot(activ, down_full, preferred_element_type=jnp.float32)  23 us
    all_gather x1, waiting for transfers between devices, body(): pieces = lax.all_gather(normed_ffn, 'tp', axis=0, tiled=True)  15.1 us
  transfers between devices with their start and end apart: 6, of which 5 were waited for; matrix products, arithmetic and copies ran while one was open for 9% of the time, Pallas kernels for 0%

commit v1 on v0

v1 whole, which is shorter than its diff:
```python
import jax
import jax.numpy as jnp
import numpy as np
from jax import lax
from jax.experimental import pallas as pl
from jax.experimental.pallas import tpu as pltpu
from jax.sharding import PartitionSpec as P

MESH = pl.DeviceIdType.MESH
HEADS = 4
DK = 128
D = 2048
BLOCK = 128
LENGTH = 1024
HALF = 512
EPS = 1e-6
C = 23
COLS = 256
LAG = 3
READY = 5 * LAG
OUT_C = 4
GU_C = 6
DOWN_C = 17
FFC = 11
F32 = jnp.float32
BF16 = jnp.bfloat16


def place():
    rep = lax.axis_index("rep")
    fs = lax.axis_index("fs")
    tp = lax.axis_index("tp")
    zl, y, x = fs // 16, (fs // 4) % 4, fs % 4
    z = rep * 2 + zl

    def dev(z_, y_, x_):
        return (z_ // 2, (z_ % 2) * 16 + y_ * 4 + x_, tp)

    xp, xm, yp, ym = (x + 1) % 4, (x + 3) % 4, (y + 1) % 4, (y + 3) % 4
    zp, zm = (z + 1) % 4, (z + 3) % 4
    to = dict(
        xp=dev(z, y, xp), xm=dev(z, y, xm), yp=dev(z, yp, x), ym=dev(z, ym, x), zp=dev(zp, y, x), zm=dev(zm, y, x)
    )
    return zl, y, x, xp, xm, yp, ym, to, (rep, fs, 1 - tp), tp


def wait_for(ref, sem):
    pltpu.make_async_copy(ref, ref, sem).wait()


def make_comm(W, send_sem, recv_sem, where):
    zl, y, x, xp, xm, yp, ym, to, partner, tp = where
    s0, s1, s2, s3 = (pl.ds(16 * i, 16) for i in range(4))
    lo, hi, al = pl.ds(0, 2), pl.ds(2, 2), slice(None)

    def put(c, stage, group, idx, d):
        r = W.at[(c,) + idx]
        pltpu.make_async_remote_copy(
            src_ref=r,
            dst_ref=r,
            send_sem=send_sem.at[group],
            recv_sem=recv_sem.at[c, stage],
            device_id=to[d],
            device_id_type=MESH,
        ).start()

    def send(c, s):
        if s == 0:
            for d in ("xp", "xm"):
                put(c, 0, 0, (zl, y, x, pl.ds(0, 32)), d)
            for d in ("yp", "ym"):
                put(c, 0, 0, (zl, y, x, pl.ds(32, 32)), d)
        elif s == 1:
            put(c, 1, 1, (zl, y, xm, s0), "xp")
            put(c, 1, 1, (zl, y, xp, s1), "xm")
            put(c, 1, 1, (zl, ym, x, s2), "yp")
            put(c, 1, 1, (zl, yp, x, s3), "ym")
        elif s == 2:
            for d in ("yp", "ym"):
                put(c, 2, 2, (zl, y, al, s0), d)
            for d in ("xp", "xm"):
                put(c, 2, 2, (zl, al, x, s2), d)
            put(c, 2, 2, (zl, y, lo, s1), "zp")
            put(c, 2, 2, (zl, y, hi, s1), "zm")
            put(c, 2, 2, (zl, lo, x, s3), "zp")
            put(c, 2, 2, (zl, hi, x, s3), "zm")
        elif s == 3:
            for d in ("yp", "ym"):
                put(c, 3, 4, (al, y, al, s1), d)
            for d in ("xp", "xm"):
                put(c, 3, 4, (al, al, x, s3), d)
            put(c, 3, 3, (zl, ym, lo, s0), "yp")
            put(c, 3, 3, (zl, yp, hi, s0), "ym")
            put(c, 3, 3, (zl, lo, xm, s2), "xp")
            put(c, 3, 3, (zl, hi, xp, s2), "xm")
        elif s == 4:
            put(c, 4, 5, (zl, lo, al, s0), "zp")
            put(c, 4, 5, (zl, hi, al, s0), "zm")
            put(c, 4, 5, (zl, al, lo, s2), "zp")
            put(c, 4, 5, (zl, al, hi, s2), "zm")
            put(c, 4, 5, (0, ym, al, s1), "yp")
            put(c, 4, 5, (1, yp, al, s1), "ym")
            put(c, 4, 5, (0, al, xm, s3), "xp")
            put(c, 4, 5, (1, al, xp, s3), "xm")

    three, two = pl.ds(0, 3), pl.ds(0, 2)

    def arrived(c, s):
        r = [
            W.at[c, 0, 0, two],
            W.at[c, 0, 0, 0],
            W.at[c, 0, three, two],
            W.at[pl.ds(0, 5), 0, 0, two],
            W.at[c, 0, three],
        ][s]
        wait_for(r, recv_sem.at[c, s])

    def drain():
        sizes = [W.at[:, 0, 0, two], W.at[:, 0, 0, 0], W.at[:, 0, three, two], W.at[:, 0, 0, two], W.at[:, :, 0], W.at[:, 0, three]]
        for i, r in enumerate(sizes):
            wait_for(r, send_sem.at[i])

    def tick(t):
        for s in range(6):
            c = t - LAG * s

            @pl.when((c >= 0) & (c < C))
            def _():
                if s:
                    arrived(c, s - 1)
                if s < 5:
                    send(c, s)

    return tick, drain


def nt(a, b):
    return lax.dot_general(a, b, (((1,), (1,)), ((), ())), preferred_element_type=F32)


def rows_normed(v, gain):
    return (v * lax.rsqrt(jnp.mean(v * v, axis=-1, keepdims=True) + EPS) * gain).astype(BF16)


def layer(
    src, tokens, mix_gain, ffn_gain, taps, cos, sin,
    out,
    W, xn, qs, ks, vs, dec, carry, hidden, mixs, mixr, pre, act, acc,
    send_sem, recv_sem, xsem, lsem,
):
    where = place()
    zl, y, x, to, partner, tp = where[0], where[1], where[2], where[7], where[8], where[9]
    other = 1 - tp
    tick, drain = make_comm(W, send_sem, recv_sem, where)
    own = pltpu.make_async_copy(src, W.at[:, zl, y, x], lsem)
    own.start()
    barrier = pltpu.get_barrier_semaphore()
    for d in list(to.values()) + [partner]:
        pl.semaphore_signal(barrier, inc=1, device_id=d, device_id_type=MESH)
    pl.semaphore_wait(barrier, 7)
    own.wait()

    def hand(src_ref, dst_ref, k):
        pltpu.make_async_remote_copy(
            src_ref=src_ref, dst_ref=dst_ref, send_sem=xsem.at[k], recv_sem=xsem.at[k + 1],
            device_id=partner, device_id_type=MESH,
        ).start()

    def rows_of(i):
        return pl.ds(pl.multiple_of(i * 128, 128), 128)

    def cols_of(n):
        return pl.ds(pl.multiple_of(n * 256, 256), 256)

    def hand_rows(i, k):
        r = xn.at[tp, rows_of(i)]
        hand(r, r, k)

    def norm_own(i):
        def one(k, _):
            r = pl.ds(pl.multiple_of(i * 128 + k * 32, 32), 32)
            xn[tp, r, :] = rows_normed(tokens[r, :].astype(F32), mix_gain[...])
            return 0

        lax.fori_loop(0, 4, one, 0)

    def tables():
        place_i = lax.broadcasted_iota(jnp.int32, (128, 128), 0).astype(F32)
        place_m = lax.broadcasted_iota(jnp.int32, (128, 128), 1).astype(F32)
        for h in range(2):
            g = jnp.full((128, 128), (tp * 2 + h).astype(F32))
            rate = (1.0 / 16.0) * jnp.exp(g * (np.log(32.0 / LENGTH) / (HEADS - 1)).astype(np.float32))
            gap = place_i - place_m
            dec[h, 0] = jnp.where(gap >= 0, jnp.exp(-jnp.maximum(gap, 0.0) * rate), 0.0)
            dec[h, 1] = jnp.exp(-(127.0 - place_i) * rate)
            dec[h, 2] = jnp.exp(-(place_i + 1.0) * rate)
            dec[h, 3] = jnp.exp(-128.0 * rate)
        pre[0:8, :] = jnp.zeros((8, 256), F32)

    def project(c, half):
        return jnp.dot(xn[half], W[c].reshape(2048, 256), preferred_element_type=F32)

    def qk_step(h):
        def one(half, _):
            u = project(2 * h, half).astype(BF16).astype(F32)
            r = pl.ds(pl.multiple_of(half * HALF, HALF), HALF)
            cs, sn = cos[r, :], sin[r, :]
            q, k = u[:, :128], u[:, 128:]
            qs[r, :] = (q * cs + pltpu.roll(q, 64, 1) * sn).astype(BF16)
            ks[r, :] = ((k * cs + pltpu.roll(k, 64, 1) * sn) * DK ** (-0.5)).astype(BF16)
            return 0

        lax.fori_loop(0, 2, one, 0)

    def v_step(h):
        def one(half, _):
            vs[pl.ds(pl.multiple_of(half * HALF, HALF), HALF), :] = project(2 * h + 1, half).astype(BF16)
            return 0

        lax.fori_loop(0, 2, one, 0)

    def retain(h):
        onset = jnp.concatenate([dec[h, 2]] * 2, axis=1)
        passing = jnp.concatenate([dec[h, 3]] * 2, axis=1)
        state = jnp.zeros((128, 256), F32)
        for b in range(8):
            r = slice(b * 128, b * 128 + 128)
            q, k, v = qs[r, :], ks[r, :], vs[r, :]
            weights = (nt(q, k) * dec[h, 0]).astype(BF16)
            ret = jnp.dot(weights, v, preferred_element_type=F32)
            if b:
                ret = ret + jnp.dot(q, state.astype(BF16), preferred_element_type=F32) * onset
            if b < 7:
                kd = (k.astype(F32) * dec[h, 1]).astype(BF16)
                fresh = lax.dot_general(kd, v, (((0,), (0,)), ((), ())), preferred_element_type=F32)
                state = state * passing + fresh if b else fresh
            cen = ret - jnp.mean(ret, axis=-1, keepdims=True)
            hidden[h, r, :] = (cen * lax.rsqrt(jnp.mean(cen * cen, axis=-1, keepdims=True) + EPS)).astype(BF16)

    def tile(c, n):
        return W[c, n // 4, n % 4].reshape(256, 256)

    def out_rows(half, n):
        r = pl.ds(pl.multiple_of(half * HALF, HALF), HALF)
        return nt(hidden[0, r, :], tile(OUT_C, n)) + nt(hidden[1, r, :], tile(OUT_C + 1, n))

    def send_cols(n, k):
        hand(mixs.at[:, cols_of(n)], mixr.at[:, cols_of(n)], k)

    def out_partner():
        def one(n, _):
            mixs[:, cols_of(n)] = out_rows(other, n).astype(BF16)

            @pl.when(n > 0)
            def _():
                send_cols(n - 1, 2)

            return 0

        lax.fori_loop(0, 8, one, 0)

    def out_own():
        def one(n, _):
            acc[0, :, cols_of(n)] = out_rows(tp, n).astype(BF16).astype(F32)

            @pl.when(n == 0)
            def _():
                send_cols(7, 2)

            return 0

        lax.fori_loop(0, 8, one, 0)

    def middle():
        wait_for(xn.at[0], xsem.at[0])
        wait_for(mixr, xsem.at[3])

        def one(i, _):
            for k in range(4):
                r = pl.ds(pl.multiple_of(i * 128 + k * 32, 32), 32)
                resid = (tokens[r, :].astype(F32) + (acc[0, r, :] + mixr[r, :].astype(F32))).astype(BF16)
                out[r, :] = resid
                xn[tp, r, :] = rows_normed(resid.astype(F32), ffn_gain[...])

            @pl.when(i > 0)
            def _():
                hand_rows(i - 1, 4)

            return 0

        lax.fori_loop(0, 4, one, 0)

    def gu_half(j, half):
        r = pl.ds(pl.multiple_of(8 + half * HALF, 8), HALF)
        pre[r, :] = project(GU_C + j, half).astype(BF16).astype(F32)

    def gu_step(j):
        gu_half(j, tp)

        @pl.when(j == 0)
        def _():
            hand_rows(3, 4)
            wait_for(xn.at[0], xsem.at[5])

        gu_half(j, other)
        k0, k1, k2 = taps[j, 0:1, :], taps[j, 1:2, :], taps[j, 2:3, :]
        lane = pl.ds(pl.multiple_of((j % 2) * 128, 128), 128)

        def one(i, _):
            u = pre[pl.ds(pl.multiple_of(i * 128, 128), 136), :]
            conv = k0 * pltpu.roll(u, 2, 0) + k1 * pltpu.roll(u, 1, 0) + k2 * u
            g, w = conv[8:, :128], conv[8:, 128:]
            act[j // 2, i // 4, pl.ds(pl.multiple_of((i % 4) * 128, 128), 128), lane] = (
                g / (1.0 + jnp.exp(-g)) * w
            ).astype(BF16)
            return 0

        lax.fori_loop(0, 8, one, 0)

    def down_first():
        def one(n, _):
            ws = [tile(DOWN_C + i, n) for i in range(4)]
            for half in range(2):
                o = nt(act[0, half], ws[0])
                for i in range(1, 4):
                    o = o + nt(act[i, half], ws[i])
                acc[half, :, cols_of(n)] = o
            return 0

        lax.fori_loop(0, 8, one, 0)

    def down_rows(half, n):
        o = acc[half, :, cols_of(n)] + nt(act[4, half], tile(DOWN_C + 4, n))
        return (o + nt(act[5, half, :, :128], tile(DOWN_C + 5, n)[:, :128])).astype(BF16)

    def down_last():
        wait_for(mixs, xsem.at[2])

        def one(n, _):
            mixs[:, cols_of(n)] = down_rows(other, n)

            @pl.when(n > 0)
            def _():
                send_cols(n - 1, 6)

            return 0

        lax.fori_loop(0, 8, one, 0)

        def two(n, _):
            acc[tp, :, cols_of(n)] = down_rows(tp, n).astype(F32)

            @pl.when(n == 0)
            def _():
                send_cols(7, 6)

            return 0

        lax.fori_loop(0, 8, two, 0)
        wait_for(mixr, xsem.at[7])

        def fin(i, _):
            r = pl.ds(pl.multiple_of(i * 32, 32), 32)
            out[r, :] = (out[r, :].astype(F32) + (acc[tp, r, :] + mixr[r, :].astype(F32))).astype(BF16)
            return 0

        lax.fori_loop(0, 16, fin, 0)
        wait_for(xn.at[0], xsem.at[4])
        wait_for(mixs, xsem.at[6])

    GU0 = READY + GU_C + 2
    LAST = READY + C - 1

    def step(t, _):
        tick(t)

        @pl.when((t >= 3) & (t < 7))
        def _():
            norm_own(t - 3)

        @pl.when((t >= 4) & (t < 8))
        def _():
            hand_rows(t - 4, 0)

        @pl.when(t == 8)
        def _():
            tables()

        @pl.when(t == READY)
        def _():
            wait_for(xn.at[0], xsem.at[1])

        @pl.when((t == READY) | (t == READY + 2))
        def _():
            qk_step((t - READY) // 2)

        @pl.when((t == READY + 1) | (t == READY + 3))
        def _():
            h = (t - READY - 1) // 2
            v_step(h)
            retain(h)

        @pl.when(t == READY + 5)
        def _():
            out_partner()

        @pl.when(t == READY + 6)
        def _():
            out_own()

        @pl.when(t == READY + 7)
        def _():
            middle()

        @pl.when((t >= GU0) & (t < GU0 + 9 + 0))
        def _():
            first = jnp.where(t < GU0 + 2, 2 * (t - GU0), t - READY - GU_C)
            count = jnp.where(t < GU0 + 2, 2, 1)
            lax.fori_loop(first, first + count, lambda j, _: (gu_step(j), 0)[1], 0)

        @pl.when(t == LAST - 2)
        def _():
            down_first()

        @pl.when(t == LAST)
        def _():
            down_last()

        return 0

    lax.fori_loop(0, LAST + 1, step, 0)
    drain()


def own_chunks(w_query, w_key, w_value, w_out, w_ffgate, w_ffup, w_down):
    parts = []
    for h in range(2):
        parts += [w_query[:, h * 128 : h * 128 + 128], w_key[:, h * 128 : h * 128 + 128]]
        parts.append(w_value[:, h * 256 : h * 256 + 256])
    parts.append(w_out.T)
    for j in range(FFC):
        parts += [w_ffgate[:, j * 128 : j * 128 + 128], w_ffup[:, j * 128 : j * 128 + 128]]
    parts += [w_down.T, jnp.zeros((64, 128), BF16)]
    flat = jnp.concatenate(parts, axis=1)
    return jnp.transpose(flat.reshape(64, C, COLS), (1, 0, 2))


def angle_tables():
    inverse = 10000.0 ** (-np.arange(64) * 2.0 / 128)
    angles = np.arange(LENGTH)[:, None] * inverse[None, :]
    cos, sin = np.cos(angles), np.sin(angles)
    return (
        np.concatenate([cos, cos], axis=1).astype(np.float32),
        np.concatenate([-sin, sin], axis=1).astype(np.float32),
    )


def body(
    tokens, mix_gain, w_query, w_key, w_value, w_out, ffn_gain, w_ffgate, w_ffup, conv_gate, conv_up, w_down
):
    tp = lax.axis_index("tp")
    src = own_chunks(w_query, w_key, w_value, w_out, w_ffgate, w_ffup, w_down)
    ff = FFC * 128
    taps = [lax.dynamic_slice_in_dim(a, tp * ff, ff, 1).reshape(3, FFC, 128) for a in (conv_gate, conv_up)]
    taps = jnp.transpose(jnp.concatenate(taps, axis=2), (1, 0, 2))
    cos, sin = angle_tables()
    vmem = pl.BlockSpec(memory_space=pltpu.VMEM)
    return pl.pallas_call(
        layer,
        out_shape=jax.ShapeDtypeStruct((HALF, D), BF16),
        in_specs=[pl.BlockSpec(memory_space=pl.ANY)] + [vmem] * 6,
        out_specs=vmem,
        scratch_shapes=[
            pltpu.VMEM((C, 2, 4, 4, 64, COLS), BF16),
            pltpu.VMEM((2, HALF, D), BF16),
            pltpu.VMEM((LENGTH, 128), BF16),
            pltpu.VMEM((LENGTH, 128), BF16),
            pltpu.VMEM((LENGTH, 256), BF16),
            pltpu.VMEM((2, 4, 128, 128), F32),
            pltpu.VMEM((8, 128), F32),
            pltpu.VMEM((2, LENGTH, 256), BF16),
            pltpu.VMEM((HALF, D), BF16),
            pltpu.VMEM((HALF, D), BF16),
            pltpu.VMEM((8 + LENGTH, 256), F32),
            pltpu.VMEM((6, 2, HALF, 256), BF16),
            pltpu.VMEM((2, HALF, D), F32),
            pltpu.SemaphoreType.DMA((6,)),
            pltpu.SemaphoreType.DMA((C, 5)),
            pltpu.SemaphoreType.DMA((8,)),
            pltpu.SemaphoreType.DMA,
        ],
        compiler_params=pltpu.CompilerParams(
            collective_id=0, has_side_effects=True, vmem_limit_bytes=67043328
        ),
    )(src, tokens, mix_gain.reshape(1, D), ffn_gain.reshape(1, D), taps, jnp.asarray(cos), jnp.asarray(sin))


def solution(mesh):
    w = P("fs", "tp")
    placed = (P(("rep", "fs", "tp"), None), P(), w, w, w, P("tp", "fs"), P(), w, w, P(), P(), P("tp", "fs"))
    return jax.shard_map(
        body, mesh=mesh, in_specs=placed, out_specs=P(("rep", "fs", "tp"), None), check_vma=False
    )
```

time: 639 us -> 151 us (0.24)
  waiting for transfers between devices: 458 us -> 0 us
  Pallas kernels: 0 us -> 122 us
  matrix products: 66.7 us -> 0 us
  blocking collectives: 55.7 us -> 0 us
  other arithmetic: 24.3 us -> 0.63 us
  local copies, waits for them, and re-layouts: 9.83 us -> 27.1 us
  between operations: 13.5 us -> 0.03 us
  starting transfers between devices: 9.54 us -> 0 us
    all_gather x5 -> x0, waiting for transfers between devices: 457 us -> none  [the longest x2 296 us: in_one_piece(): out, at, done = (lax.all_gather(both, axis, axis=dim, tiled=True), 0, [])]
    pallas_call x0 -> x1, Pallas kernels: none -> 122 us  [body(): pl.pallas_call(layer, out_shape=jax.ShapeDtypeStruct((HALF, D), BF16), in...]
    dot_general x10 -> x0, matrix products: 66.7 us -> none  [the longest x1 23 us: body(): jnp.dot(activ, down_full, preferred_element_type=jnp.float32)]
    all_to_all x2 -> x0, blocking collectives: 55.7 us -> none  [sent_and_summed(): lax.all_to_all(in_blocks(shard, dim, length), axis, 0, 0, tiled=True)]
    unnamed x32 -> x31, local copies, waits for them, and re-layouts: 3.79 us -> 25.3 us
    all_to_all x1 -> x0, starting transfers between devices: 9.34 us -> none  [copy_for_each(): lax.all_to_all(jnp.broadcast_to(shard[None], (length, *shard.shape)), axi...]
    convert_element_type x7 -> x0, other arithmetic: 8.85 us -> none  [the longest x2 5.33 us: rms_rows(): return (values * factor * scale_vec).astype(jnp.bfloat16)]
  transfers between devices with their start and end apart: 6 -> 0, of which waited for: 5 -> 0; matrix products, arithmetic and copies ran while one was open for 9% -> 0% of each run, Pallas kernels for 0% -> 0%
where the time goes in v1:
time: 151 us; the launch traced here: 150 us
  Pallas kernels  122 us (81%)
  local copies, waits for them, and re-layouts  27.1 us (18%)
    pallas_call x1, Pallas kernels, body(): pl.pallas_call(layer, out_shape=jax.ShapeDtypeStruct((HALF, D), BF16), in...  122 us
    unnamed x31, local copies, waits for them, and re-layouts  25.3 us

profile of v1, /device:TPU:1, one launch (start us, length us, event | category | flops | bytes accessed | tf_op | source)
XLA Modules:
  0.0 149.5 jit_solution(16668181677586334133)
XLA Ops:
  0.0 0.8 dynamic-slice_bitcast_fusion
  0.8 0.6 maximum_bitcast_fusion.taps
  1.4 0.7 constant_dynamic-update-slice_fusion.29
  2.1 0.7 constant_dynamic-update-slice_fusion.28
  2.8 0.8 constant_dynamic-update-slice_fusion.27
  3.6 0.7 constant_dynamic-update-slice_fusion.26
  4.3 0.7 constant_dynamic-update-slice_fusion.25
  5.0 0.8 constant_dynamic-update-slice_fusion.24
  5.8 0.8 constant_dynamic-update-slice_fusion.23
  6.7 0.7 constant_dynamic-update-slice_fusion.22
  7.4 0.7 constant_dynamic-update-slice_fusion.21
  8.1 0.7 constant_dynamic-update-slice_fusion.20
  8.8 0.7 constant_dynamic-update-slice_fusion.19
  9.6 0.7 constant_dynamic-update-slice_fusion.18
  10.3 0.7 constant_dynamic-update-slice_fusion.17
  11.0 0.7 constant_dynamic-update-slice_fusion.16
  11.7 0.7 constant_dynamic-update-slice_fusion.15
  12.5 0.7 constant_dynamic-update-slice_fusion.14
  13.2 0.7 constant_dynamic-update-slice_fusion.13
  13.9 0.7 constant_dynamic-update-slice_fusion.12
  14.6 0.7 constant_dynamic-update-slice_fusion.11
  15.4 0.7 constant_dynamic-update-slice_fusion.10
  16.1 0.7 constant_dynamic-update-slice_fusion.9
  16.8 0.7 constant_dynamic-update-slice_fusion.8
  17.5 0.7 constant_dynamic-update-slice_fusion.7
  18.3 0.7 constant_dynamic-update-slice_fusion.6
  19.0 0.7 constant_dynamic-update-slice_fusion.5
  19.7 0.7 constant_dynamic-update-slice_fusion.4
  20.5 0.7 constant_dynamic-update-slice_fusion.3
  21.2 0.7 constant_dynamic-update-slice_fusion.2
  21.9 0.7 constant_dynamic-update-slice_fusion.1
  22.6 0.9 bitcast_dynamic-update-slice_fusion
  23.6 1.0 copy.18
  24.5 121.8 %shard_map.136 = bf16[512,2048]{1,0:T(8,128)(2,1)} custom-call(bf16[23,64,256]{2,1,0:T(8,128)(2,1)} %bitcast.19, bf16[512,2048]{1,0:T(8,128)(2,1)} %tokens.1, f32[1,2048]{1,0:T(1,128)} %bitcast.21, f32[1,2048]{1,0:T(1,128)} %bitcast.22, f32[11,3,256]{2,1,0:T(4,128)} %maximum_bitcast_fusion.taps, f32[1024,128]{1,0:T(8,128)} %constant.16.clone.cos, ...), custom_call_target="tpu_custom_call" | custom-call | tf_op jit(solution)/shard_map/pallas_call | solution.py:468
  146.3 3.2 %copy.50 = bf16[512,2048]{1,0:T(8,128)(2,1)} copy(bf16[512,2048]{1,0:T(8,128)(2,1)} %shard_map.136) | data formatting | bytes 4194304
  (1 shorter events, 0.0 us)

commit v2 on v1

v2 whole, which is shorter than its diff:
```python
import jax
import jax.numpy as jnp
import numpy as np
from jax import lax
from jax.experimental import pallas as pl
from jax.experimental.pallas import tpu as pltpu
from jax.sharding import PartitionSpec as P

MESH = pl.DeviceIdType.MESH
HEADS = 4
DK = 128
D = 2048
BLOCK = 128
LENGTH = 1024
HALF = 512
EPS = 1e-6
C = 23
COLS = 256
LAG = 3
READY = 3 * LAG
FULL = 22
VLIM = 67043328
NORM = 20
GROUPS = ((0, 2), (2, 6), (6, 14), (14, 22), (22, 23))
OUT_C = 4
GU_C = 6
DOWN_C = 17
FFC = 11
F32 = jnp.float32
BF16 = jnp.bfloat16


def place():
    rep = lax.axis_index("rep")
    fs = lax.axis_index("fs")
    tp = lax.axis_index("tp")
    zl, y, x = fs // 16, (fs // 4) % 4, fs % 4
    z = rep * 2 + zl

    def dev(z_, y_, x_):
        return (z_ // 2, (z_ % 2) * 16 + y_ * 4 + x_, tp)

    xp, xm, yp, ym = (x + 1) % 4, (x + 3) % 4, (y + 1) % 4, (y + 3) % 4
    zp, zm = (z + 1) % 4, (z + 3) % 4
    to = dict(
        xp=dev(z, y, xp), xm=dev(z, y, xm), yp=dev(z, yp, x), ym=dev(z, ym, x), zp=dev(zp, y, x), zm=dev(zm, y, x)
    )
    return zl, y, x, xp, xm, yp, ym, to, (rep, fs, 1 - tp), tp


def wait_for(ref, sem):
    pltpu.make_async_copy(ref, ref, sem).wait()


def make_comm(W, send_sem, recv_sem, early_sem, where):
    zl, y, x, xp, xm, yp, ym, to, partner, tp = where
    s0, s1, s2, s3 = (pl.ds(16 * i, 16) for i in range(4))
    lo, hi, al = pl.ds(0, 2), pl.ds(2, 2), slice(None)
    two, three = pl.ds(0, 2), pl.ds(0, 3)

    def put(r, sem, recv, d):
        pltpu.make_async_remote_copy(
            src_ref=r, dst_ref=r, send_sem=sem, recv_sem=recv, device_id=to[d], device_id_type=MESH
        ).start()

    def lanes_of(half):
        return pl.ds(0, 128) if half else pl.ds(0, 256)

    def early(g, s):
        c0, c1 = GROUPS[g]
        cs, lanes = pl.ds(c0, c1 - c0), lanes_of(c0 == FULL)
        sem, recv = early_sem.at[g, s], early_sem.at[g, 2 + s]
        if s == 0:
            for d in ("xp", "xm"):
                put(W.at[cs, zl, y, x, pl.ds(0, 32), lanes], sem, recv, d)
            for d in ("yp", "ym"):
                put(W.at[cs, zl, y, x, pl.ds(32, 32), lanes], sem, recv, d)
        else:
            put(W.at[cs, zl, y, xm, s0, lanes], sem, recv, "xp")
            put(W.at[cs, zl, y, xp, s1, lanes], sem, recv, "xm")
            put(W.at[cs, zl, ym, x, s2, lanes], sem, recv, "yp")
            put(W.at[cs, zl, yp, x, s3, lanes], sem, recv, "ym")

    def early_ref(g, s):
        c0, c1 = GROUPS[g]
        cs, lanes = pl.ds(c0, c1 - c0), lanes_of(c0 == FULL)
        return W.at[cs, 0, 0, two if s == 0 else pl.ds(0, 1), :, lanes]

    def early_arrived(g, s):
        wait_for(early_ref(g, s), early_sem.at[g, 2 + s])

    def send(c, s):
        def go(group, idx, d):
            put(W.at[(c,) + idx], send_sem.at[group], recv_sem.at[c, s - 2], d)

        if s == 2:
            for d in ("yp", "ym"):
                go(0, (zl, y, al, s0), d)
            for d in ("xp", "xm"):
                go(0, (zl, al, x, s2), d)
            go(0, (zl, y, lo, s1), "zp")
            go(0, (zl, y, hi, s1), "zm")
            go(0, (zl, lo, x, s3), "zp")
            go(0, (zl, hi, x, s3), "zm")
        elif s == 3:
            for d in ("yp", "ym"):
                go(2, (al, y, al, s1), d)
            for d in ("xp", "xm"):
                go(2, (al, al, x, s3), d)
            go(1, (zl, ym, lo, s0), "yp")
            go(1, (zl, yp, hi, s0), "ym")
            go(1, (zl, lo, xm, s2), "xp")
            go(1, (zl, hi, xp, s2), "xm")
        elif s == 4:
            go(3, (zl, lo, al, s0), "zp")
            go(3, (zl, hi, al, s0), "zm")
            go(3, (zl, al, lo, s2), "zp")
            go(3, (zl, al, hi, s2), "zm")
            go(3, (0, ym, al, s1), "yp")
            go(3, (1, yp, al, s1), "ym")
            go(3, (0, al, xm, s3), "xp")
            go(3, (1, al, xp, s3), "xm")

    top, low = pl.ds(0, 32), pl.ds(32, 32)

    def send_late(c, s, half):
        def go(idx, d):
            put(W.at[(c,) + idx + (lanes_of(half),)], send_sem.at[4 + 3 * half + s - 2], recv_sem.at[c, s - 2], d)

        if s == 2:
            go((zl, y, lo, top), "zp")
            go((zl, y, hi, top), "zm")
            go((zl, lo, x, low), "zp")
            go((zl, hi, x, low), "zm")
        elif s == 3:
            for d in ("yp", "ym"):
                go((al, y, al, top), d)
            for d in ("xp", "xm"):
                go((al, al, x, low), d)
        elif s == 4:
            go((0, ym, al, top), "yp")
            go((1, yp, al, top), "ym")
            go((0, al, xm, low), "xp")
            go((1, al, xp, low), "xm")

    def late_refs(cs, half):
        ln = lanes_of(half)
        return [W.at[cs, 0, 0, :, :, ln], W.at[cs, 0, :, :, :, ln], W.at[cs, :, 0, :, :, ln]]

    def arrived(c, s):
        r = [W.at[c, 0, three, two], W.at[pl.ds(0, 5), 0, 0, two], W.at[c, 0, three]][s - 2]
        wait_for(r, recv_sem.at[c, s - 2])

    def drain():
        for g in range(len(GROUPS)):
            for s in range(2):
                wait_for(early_ref(g, s), early_sem.at[g, s])
        cs = pl.ds(0, NORM)
        for i, r in enumerate([W.at[cs, 0, three, two], W.at[cs, 0, 0, two], W.at[cs, :, 0], W.at[cs, 0, three]]):
            wait_for(r, send_sem.at[i])
        for half in range(2):
            for i, r in enumerate(late_refs(pl.ds(FULL, 1) if half else pl.ds(NORM, FULL - NORM), half)):
                wait_for(r, send_sem.at[4 + 3 * half + i])

    def tick(t):
        for s in range(2, 6):
            c = t - LAG * (s - 2)

            @pl.when((c >= 0) & (c < NORM))
            def _():
                if s > 2:
                    arrived(c, s - 1)
                if s < 5:
                    send(c, s)

            def late(half):
                if s > 2:
                    wait_for(late_refs(c, half)[s - 3], recv_sem.at[c, s - 3])
                if s < 5:
                    send_late(c, s, half)

            @pl.when((c >= NORM) & (c < FULL))
            def _():
                late(0)

            @pl.when(c == FULL)
            def _():
                late(1)

    return tick, drain, early, early_arrived


def nt(a, b):
    return lax.dot_general(a, b, (((1,), (1,)), ((), ())), preferred_element_type=F32)


def rows_normed(v, gain):
    return (v * lax.rsqrt(jnp.mean(v * v, axis=-1, keepdims=True) + EPS) * gain).astype(BF16)


def layer(
    w_query, w_key, w_value, w_outt, w_ffgate, w_ffup, w_downt,
    tokens_in, cos_in, sin_in, mix_gain, ffn_gain, tap_gate, tap_up,
    out,
    W, tokens, cos, sin, xn, qs, ks, vs, dec, hidden, mixs, mixr, pre_a, pre_b, act, acc,
    send_sem, recv_sem, early_sem, xsem, lsem, fsem,
):
    where = place()
    zl, y, x, to, partner, tp = where[0], where[1], where[2], where[7], where[8], where[9]
    other = 1 - tp
    tick, drain, early, early_arrived = make_comm(W, send_sem, recv_sem, early_sem, where)

    def load(ref, c, lanes, g):
        pltpu.make_async_copy(ref, W.at[c, zl, y, x, :, lanes], lsem.at[g]).start()

    own_rows = [pltpu.make_async_copy(a, b, lsem.at[k]) for a, b, k in ((tokens_in, tokens, 5), (cos_in, cos, 6), (sin_in, sin, 7))]
    own_rows[0].start()
    left, right, whole = pl.ds(0, 128), pl.ds(128, 128), pl.ds(0, 256)
    for h in range(2):
        load(w_query.at[:, pl.ds(h * 128, 128)], 2 * h, left, h)
        load(w_key.at[:, pl.ds(h * 128, 128)], 2 * h, right, h)
        load(w_value.at[:, pl.ds(h * 256, 256)], 2 * h + 1, whole, h)
    for i in range(2):
        load(w_outt.at[:, pl.ds(i * 256, 256)], OUT_C + i, whole, 1)
    for j in range(FFC):
        g = 2 if GU_C + j < GROUPS[2][1] else 3
        load(w_ffgate.at[:, pl.ds(j * 128, 128)], GU_C + j, left, g)
        load(w_ffup.at[:, pl.ds(j * 128, 128)], GU_C + j, right, g)
    for i in range(5):
        load(w_downt.at[:, pl.ds(i * 256, 256)], DOWN_C + i, whole, 3)
    load(w_downt.at[:, pl.ds(1280, 128)], FULL, left, 4)
    own_rows[1].start()
    own_rows[2].start()

    def loaded(g):
        c0, c1 = GROUPS[g]
        wait_for(W.at[pl.ds(c0, c1 - c0), zl, y, x, :, left if g == 4 else whole], lsem.at[g])

    barrier = pltpu.get_barrier_semaphore()
    for d in list(to.values()) + [partner]:
        pl.semaphore_signal(barrier, inc=1, device_id=d, device_id_type=MESH)
    pl.semaphore_wait(barrier, 7)

    def hand(src_ref, dst_ref, k):
        pltpu.make_async_remote_copy(
            src_ref=src_ref, dst_ref=dst_ref, send_sem=xsem.at[k], recv_sem=xsem.at[k + 1],
            device_id=partner, device_id_type=MESH,
        ).start()

    def rows_of(i):
        return pl.ds(pl.multiple_of(i * 128, 128), 128)

    def cols_of(n):
        return pl.ds(pl.multiple_of(n * 256, 256), 256)

    def hand_rows(i, k):
        r = xn.at[tp, rows_of(i)]
        hand(r, r, k)

    def norm_own(i):
        def one(k, _):
            r = pl.ds(pl.multiple_of(i * 128 + k * 32, 32), 32)
            xn[tp, r, :] = rows_normed(tokens[r, :].astype(F32), mix_gain[...])
            return 0

        lax.fori_loop(0, 4, one, 0)

    def tables():
        place_i = lax.broadcasted_iota(jnp.int32, (128, 128), 0).astype(F32)
        place_m = lax.broadcasted_iota(jnp.int32, (128, 128), 1).astype(F32)
        for h in range(2):
            g = jnp.full((128, 128), (tp * 2 + h).astype(F32))
            rate = (1.0 / 16.0) * jnp.exp(g * (np.log(32.0 / LENGTH) / (HEADS - 1)).astype(np.float32))
            gap = place_i - place_m
            dec[h, 0] = jnp.where(gap >= 0, jnp.exp(-jnp.maximum(gap, 0.0) * rate), 0.0)
            dec[h, 1] = jnp.exp(-(127.0 - place_i) * rate)
            dec[h, 2] = jnp.exp(-(place_i + 1.0) * rate)
            dec[h, 3] = jnp.exp(-128.0 * rate)
        pre_a[0:8, :] = jnp.zeros((8, 256), F32)

        def clear(i, _):
            pre_b[pl.ds(pl.multiple_of(i * 8, 8), 8), :] = jnp.zeros((8, 256), F32)
            return 0

        lax.fori_loop(0, (8 + LENGTH) // 8, clear, 0)

    def project(c, half):
        return jnp.dot(xn[half], W[c].reshape(2048, 256), preferred_element_type=F32)

    def qk_step(h):
        def one(half, _):
            u = project(2 * h, half).astype(BF16).astype(F32)
            r = pl.ds(pl.multiple_of(half * HALF, HALF), HALF)
            cs, sn = cos[r, :], sin[r, :]
            q, k = u[:, :128], u[:, 128:]
            qs[r, :] = (q * cs + pltpu.roll(q, 64, 1) * sn).astype(BF16)
            ks[r, :] = ((k * cs + pltpu.roll(k, 64, 1) * sn) * DK ** (-0.5)).astype(BF16)
            return 0

        lax.fori_loop(0, 2, one, 0)

    def v_step(h):
        def one(half, _):
            vs[pl.ds(pl.multiple_of(half * HALF, HALF), HALF), :] = project(2 * h + 1, half).astype(BF16)
            return 0

        lax.fori_loop(0, 2, one, 0)

    def retain(h):
        onset = jnp.concatenate([dec[h, 2]] * 2, axis=1)
        passing = jnp.concatenate([dec[h, 3]] * 2, axis=1)
        state = jnp.zeros((128, 256), F32)
        for b in range(8):
            r = slice(b * 128, b * 128 + 128)
            q, k, v = qs[r, :], ks[r, :], vs[r, :]
            weights = (nt(q, k) * dec[h, 0]).astype(BF16)
            ret = jnp.dot(weights, v, preferred_element_type=F32)
            if b:
                ret = ret + jnp.dot(q, state.astype(BF16), preferred_element_type=F32) * onset
            if b < 7:
                kd = (k.astype(F32) * dec[h, 1]).astype(BF16)
                fresh = lax.dot_general(kd, v, (((0,), (0,)), ((), ())), preferred_element_type=F32)
                state = state * passing + fresh if b else fresh
            cen = ret - jnp.mean(ret, axis=-1, keepdims=True)
            hidden[h, r, :] = (cen * lax.rsqrt(jnp.mean(cen * cen, axis=-1, keepdims=True) + EPS)).astype(BF16)

    def tile(c, n):
        return W[c, n // 4, n % 4].reshape(256, 256)

    def out_rows(half, n):
        r = pl.ds(pl.multiple_of(half * HALF, HALF), HALF)
        return nt(hidden[0, r, :], tile(OUT_C, n)) + nt(hidden[1, r, :], tile(OUT_C + 1, n))

    def send_cols(n, k):
        hand(mixs.at[:, cols_of(n)], mixr.at[:, cols_of(n)], k)

    def out_partner():
        def one(n, _):
            mixs[:, cols_of(n)] = out_rows(other, n).astype(BF16)

            @pl.when(n > 0)
            def _():
                send_cols(n - 1, 2)

            return 0

        lax.fori_loop(0, 8, one, 0)

    def out_own():
        def one(n, _):
            acc[0, :, cols_of(n)] = out_rows(tp, n).astype(BF16).astype(F32)

            @pl.when(n == 0)
            def _():
                send_cols(7, 2)

            return 0

        lax.fori_loop(0, 8, one, 0)

    def middle():
        wait_for(xn.at[0], xsem.at[0])
        wait_for(mixr, xsem.at[3])

        def one(i, _):
            for k in range(4):
                r = pl.ds(pl.multiple_of(i * 128 + k * 32, 32), 32)
                resid = (tokens[r, :].astype(F32) + (acc[0, r, :] + mixr[r, :].astype(F32))).astype(BF16)
                out[r, :] = resid
                xn[tp, r, :] = rows_normed(resid.astype(F32), ffn_gain[...])

            @pl.when(i > 0)
            def _():
                hand_rows(i - 1, 4)

            return 0

        lax.fori_loop(0, 4, one, 0)

    def gu_dot(j, half, pre):
        r = pl.ds(pl.multiple_of(8 + half * HALF, 8), HALF)
        pre[r, :] = project(GU_C + j, half).astype(BF16).astype(F32)

    def gu_conv(j, half, pre):
        mine = pl.ds(pl.multiple_of(tp * (FFC * 128) + j * 128, 128), 128)
        k0, k1, k2 = (
            jnp.concatenate([tap_gate[k : k + 1, mine], tap_up[k : k + 1, mine]], axis=1) for k in range(3)
        )
        lane = pl.ds(pl.multiple_of((j % 2) * 128, 128), 128)
        for i in range(8):
            u = pre[pl.ds(pl.multiple_of(half * HALF + i * 64, 64), 72), :]
            conv = k0 * pltpu.roll(u, 2, 0) + k1 * pltpu.roll(u, 1, 0) + k2 * u
            g, w = conv[8:, :128], conv[8:, 128:]
            act[j // 2, half, i * 64 : i * 64 + 64, lane] = (g / (1.0 + jnp.exp(-g)) * w).astype(BF16)

    def gu_step(j, now, before):
        last = jnp.maximum(j - 1, 0)
        gu_dot(j, tp, now)
        gu_conv(last, tp, before)

        @pl.when(j == 0)
        def _():
            hand_rows(3, 4)
            wait_for(xn.at[0], xsem.at[5])

        gu_dot(j, other, now)
        gu_conv(last, other, before)

    def down_first(n0):
        def one(n, _):
            ws = [tile(DOWN_C + i, n) for i in range(4)]
            for half in range(2):
                o = nt(act[0, half], ws[0])
                for i in range(1, 4):
                    o = o + nt(act[i, half], ws[i])
                acc[half, :, cols_of(n)] = o
            return 0

        lax.fori_loop(n0, n0 + 4, one, 0)

    def down_rows(half, n):
        o = acc[half, :, cols_of(n)] + nt(act[4, half], tile(DOWN_C + 4, n))
        return (o + nt(act[5, half, :, :128], tile(DOWN_C + 5, n)[:, :128])).astype(BF16)

    def send_piece(n):
        pltpu.make_async_remote_copy(
            src_ref=mixs.at[:, cols_of(n)], dst_ref=mixr.at[:, cols_of(n)], send_sem=xsem.at[6], recv_sem=fsem.at[n],
            device_id=partner, device_id_type=MESH,
        ).start()

    def down_last():
        wait_for(mixs, xsem.at[2])

        def one(n, _):
            mixs[:, cols_of(n)] = down_rows(other, n)

            @pl.when(n > 0)
            def _():
                send_piece(n - 1)

            return 0

        lax.fori_loop(0, 8, one, 0)

        def two(n, _):
            mine = down_rows(tp, n).astype(F32)

            @pl.when(n == 0)
            def _():
                send_piece(7)

            wait_for(mixr.at[:, pl.ds(0, 256)], fsem.at[n])
            out[:, cols_of(n)] = (
                out[:, cols_of(n)].astype(F32) + (mine + mixr[:, cols_of(n)].astype(F32))
            ).astype(BF16)
            return 0

        lax.fori_loop(0, 8, two, 0)
        wait_for(xn.at[0], xsem.at[4])
        wait_for(mixs, xsem.at[6])

    GU0 = READY + GU_C + 2
    NORM0 = READY - 5
    LAST = READY + C - 1

    loaded(0)
    early(0, 0)
    loaded(1)
    early(1, 0)
    early_arrived(0, 0)
    early(0, 1)
    loaded(2)
    early(2, 0)
    early_arrived(1, 0)
    early(1, 1)

    def step(t, _):
        for g in (0, 1, 2, 3, 4):
            @pl.when(t == GROUPS[g][0])
            def _():
                early_arrived(g, 1)

        tick(t)

        @pl.when(t == 1)
        def _():
            for g in (3, 4):
                loaded(g)
                early(g, 0)

        @pl.when(t == 2)
        def _():
            early_arrived(2, 0)
            early(2, 1)

        @pl.when(t == 4)
        def _():
            for g in (3, 4):
                early_arrived(g, 0)
                early(g, 1)

        @pl.when(t == NORM0)
        def _():
            own_rows[0].wait()

        @pl.when((t >= NORM0) & (t < NORM0 + 4))
        def _():
            norm_own(t - NORM0)

        @pl.when((t > NORM0) & (t <= NORM0 + 4))
        def _():
            hand_rows(t - NORM0 - 1, 0)

        @pl.when(t == NORM0 - 1)
        def _():
            tables()

        @pl.when(t == READY)
        def _():
            own_rows[1].wait()
            own_rows[2].wait()
            wait_for(xn.at[0], xsem.at[1])

        @pl.when((t == READY) | (t == READY + 2))
        def _():
            qk_step((t - READY) // 2)

        @pl.when((t == READY + 1) | (t == READY + 3))
        def _():
            v_step((t - READY - 1) // 2)

        @pl.when((t == READY + 1) | (t == READY + 4))
        def _():
            retain((t - READY - 1) // 3)

        @pl.when(t == READY + 5)
        def _():
            out_partner()

        @pl.when(t == READY + 6)
        def _():
            out_own()

        @pl.when(t == READY + 7)
        def _():
            middle()

        @pl.when((t >= GU0) & (t < GU0 + FFC) & ((t - GU0) % 2 == 0))
        def _():
            gu_step(t - GU0, pre_a, pre_b)

        @pl.when((t >= GU0) & (t < GU0 + FFC) & ((t - GU0) % 2 == 1))
        def _():
            gu_step(t - GU0, pre_b, pre_a)

        @pl.when(t == GU0 + FFC)
        def _():
            lax.fori_loop(0, 2, lambda half, _: (gu_conv(FFC - 1, half, pre_a), 0)[1], 0)

        @pl.when((t == LAST - 2) | (t == LAST - 1))
        def _():
            down_first(4 * (t - LAST + 2))

        @pl.when(t == LAST)
        def _():
            down_last()

        return 0

    lax.fori_loop(0, LAST + 1, step, 0)
    drain()


def angle_tables():
    inverse = 10000.0 ** (-np.arange(64) * 2.0 / 128)
    angles = np.arange(LENGTH)[:, None] * inverse[None, :]
    cos, sin = np.cos(angles), np.sin(angles)
    return (
        np.concatenate([cos, cos], axis=1).astype(np.float32),
        np.concatenate([-sin, sin], axis=1).astype(np.float32),
    )


def body(
    tokens, mix_gain, w_query, w_key, w_value, w_out, ffn_gain, w_ffgate, w_ffup, conv_gate, conv_up, w_down
):
    cos, sin = angle_tables()
    vmem = pl.BlockSpec(memory_space=pltpu.VMEM)
    hbm = pl.BlockSpec(memory_space=pl.ANY)
    whole = jax.ShapeDtypeStruct((HALF, D), BF16)
    return pl.pallas_call(
        layer,
        out_shape=whole,
        in_specs=[hbm] * 10 + [vmem] * 4,
        out_specs=vmem,
        scratch_shapes=[
            pltpu.VMEM((C, 2, 4, 4, 64, COLS), BF16),
            pltpu.VMEM((HALF, D), BF16),
            pltpu.VMEM((LENGTH, 128), F32),
            pltpu.VMEM((LENGTH, 128), F32),
            pltpu.VMEM((2, HALF, D), BF16),
            pltpu.VMEM((LENGTH, 128), BF16),
            pltpu.VMEM((LENGTH, 128), BF16),
            pltpu.VMEM((LENGTH, 256), BF16),
            pltpu.VMEM((2, 4, 128, 128), F32),
            pltpu.VMEM((2, LENGTH, 256), BF16),
            pltpu.VMEM((HALF, D), BF16),
            pltpu.VMEM((HALF, D), BF16),
            pltpu.VMEM((8 + LENGTH, 256), F32),
            pltpu.VMEM((8 + LENGTH, 256), F32),
            pltpu.VMEM((6, 2, HALF, 256), BF16),
            pltpu.VMEM((2, HALF, D), F32),
            pltpu.SemaphoreType.DMA((10,)),
            pltpu.SemaphoreType.DMA((C, 3)),
            pltpu.SemaphoreType.DMA((len(GROUPS), 4)),
            pltpu.SemaphoreType.DMA((8,)),
            pltpu.SemaphoreType.DMA((8,)),
            pltpu.SemaphoreType.DMA((8,)),
        ],
        compiler_params=pltpu.CompilerParams(
            collective_id=0, has_side_effects=True, vmem_limit_bytes=VLIM
        ),
    )(
        w_query, w_key, w_value, w_out.T, w_ffgate, w_ffup, w_down.T,
        tokens, jnp.asarray(cos), jnp.asarray(sin), mix_gain.reshape(1, D), ffn_gain.reshape(1, D), conv_gate, conv_up,
    )


def solution(mesh):
    w = P("fs", "tp")
    placed = (P(("rep", "fs", "tp"), None), P(), w, w, w, P("tp", "fs"), P(), w, w, P(), P(), P("tp", "fs"))
    return jax.shard_map(
        body, mesh=mesh, in_specs=placed, out_specs=P(("rep", "fs", "tp"), None), check_vma=False
    )
```

time: 151 us -> 118 us (0.78)
  local copies, waits for them, and re-layouts: 27.1 us -> 3.16 us
  Pallas kernels: 122 us -> 115 us
    unnamed x31 -> x1, local copies, waits for them, and re-layouts: 25.3 us -> 3.16 us
    pallas_call x1, Pallas kernels: 122 us -> 115 us  [body(): pl.pallas_call(layer, out_shape=whole, in_specs=[hbm] * 10 + [vmem] * 4,...]
    reshape x2 -> x0, local copies, waits for them, and re-layouts: 1.71 us -> none  [the longest x1 0.96 us: own_chunks(): return jnp.transpose(flat.reshape(64, C, COLS), (1, 0, 2))]
where the time goes in v2:
time: 118 us
  Pallas kernels  115 us (97%)
  local copies, waits for them, and re-layouts  3.16 us (3%)
    pallas_call x1, Pallas kernels, body(): pl.pallas_call(layer, out_shape=whole, in_specs=[hbm] * 10 + [vmem] * 4,...  115 us
    unnamed x1, local copies, waits for them, and re-layouts  3.16 us

profile of v2, /device:TPU:1, one launch (start us, length us, event | category | flops | bytes accessed | tf_op | source)
XLA Modules:
  0.0 117.8 jit_solution(5240746517184565244)
XLA Ops:
  0.0 114.6 %shard_map.136 = bf16[512,2048]{1,0:T(8,128)(2,1)} custom-call(bf16[64,256]{1,0:T(8,128)(2,1)} %w_query.1, bf16[64,256]{1,0:T(8,128)(2,1)} %w_key.1, bf16[64,512]{1,0:T(8,128)(2,1)} %w_value.1, bf16[64,512]{1,0:T(8,128)(2,1)} %bitcast.5, bf16[64,1408]{1,0:T(8,128)(2,1)} %w_ffgate.1, bf16[64,1408]{1,0:T(8,128)(2,1)} %w_ffup.1, bf16[64,1408]{1,0:T(8,128)(2,1)} %bitcast.4, ...), custom_call_target="tpu_custom_call" | custom-call | tf_op jit(solution)/shard_map/pallas_call | solution.py:591
  114.6 3.2 %copy.16 = bf16[512,2048]{1,0:T(8,128)(2,1)} copy(bf16[512,2048]{1,0:T(8,128)(2,1)} %shard_map.136) | data formatting | bytes 4194304

commit v3 on v2

--- a/solution.py
+++ b/solution.py
@@ -201,9 +201,9 @@
 def layer(
     w_query, w_key, w_value, w_outt, w_ffgate, w_ffup, w_downt,
     tokens_in, cos_in, sin_in, mix_gain, ffn_gain, tap_gate, tap_up,
-    out,
-    W, tokens, cos, sin, xn, qs, ks, vs, dec, hidden, mixs, mixr, pre_a, pre_b, act, acc,
-    send_sem, recv_sem, early_sem, xsem, lsem, fsem,
+    out_hbm,
+    W, out, tokens, cos, sin, xn, qs, ks, vs, dec, hidden, mixs, mixr, pre_a, pre_b, act, acc,
+    send_sem, recv_sem, early_sem, xsem, lsem, fsem, osem,
 ):
     where = place()
     zl, y, x, to, partner, tp = where[0], where[1], where[2], where[7], where[8], where[9]
@@ -406,21 +406,22 @@
         gu_dot(j, other, now)
         gu_conv(last, other, before)
 
-    def down_first(n0):
-        def one(n, _):
-            ws = [tile(DOWN_C + i, n) for i in range(4)]
-            for half in range(2):
-                o = nt(act[0, half], ws[0])
-                for i in range(1, 4):
-                    o = o + nt(act[i, half], ws[i])
-                acc[half, :, cols_of(n)] = o
-            return 0
-
-        lax.fori_loop(n0, n0 + 4, one, 0)
+    def down_part(first, count):
+        def one(i, _):
+            for k in range(2):
+                n = 2 * i + k
+                for half in range(2):
+                    o = nt(act[first, half], tile(DOWN_C + first, n))
+                    for d in range(1, count):
+                        o = o + nt(act[first + d, half], tile(DOWN_C + first + d, n))
+                    acc[half, :, cols_of(n)] = acc[half, :, cols_of(n)] + o if first else o
+            return 0
+
+        lax.fori_loop(0, 4, one, 0)
 
     def down_rows(half, n):
-        o = acc[half, :, cols_of(n)] + nt(act[4, half], tile(DOWN_C + 4, n))
-        return (o + nt(act[5, half, :, :128], tile(DOWN_C + 5, n)[:, :128])).astype(BF16)
+        o = acc[half, :, cols_of(n)] + nt(act[5, half, :, :128], tile(DOWN_C + 5, n)[:, :128])
+        return o.astype(BF16)
 
     def send_piece(n):
         pltpu.make_async_remote_copy(
@@ -428,34 +429,49 @@
             device_id=partner, device_id_type=MESH,
         ).start()
 
+    def put_out(i):
+        c = pl.ds(pl.multiple_of(i * 512, 512), 512)
+        return pltpu.make_async_copy(out.at[:, c], out_hbm.at[:, c], osem)
+
     def down_last():
         wait_for(mixs, xsem.at[2])
 
-        def one(n, _):
-            mixs[:, cols_of(n)] = down_rows(other, n)
-
-            @pl.when(n > 0)
-            def _():
-                send_piece(n - 1)
-
-            return 0
-
-        lax.fori_loop(0, 8, one, 0)
-
-        def two(n, _):
-            mine = down_rows(tp, n).astype(F32)
-
-            @pl.when(n == 0)
-            def _():
+        def one(i, _):
+            for k in range(2):
+                mixs[:, cols_of(2 * i + k)] = down_rows(other, 2 * i + k)
+
+            @pl.when(i > 0)
+            def _():
+                send_piece(2 * i - 2)
+                send_piece(2 * i - 1)
+
+            return 0
+
+        lax.fori_loop(0, 4, one, 0)
+
+        def two(i, _):
+            mine = [down_rows(tp, 2 * i + k).astype(F32) for k in range(2)]
+
+            @pl.when(i == 0)
+            def _():
+                send_piece(6)
                 send_piece(7)
 
-            wait_for(mixr.at[:, pl.ds(0, 256)], fsem.at[n])
-            out[:, cols_of(n)] = (
-                out[:, cols_of(n)].astype(F32) + (mine + mixr[:, cols_of(n)].astype(F32))
-            ).astype(BF16)
-            return 0
-
-        lax.fori_loop(0, 8, two, 0)
+            for k in range(2):
+                n = 2 * i + k
+                wait_for(mixr.at[:, pl.ds(0, 256)], fsem.at[n])
+                out[:, cols_of(n)] = (
+                    out[:, cols_of(n)].astype(F32) + (mine[k] + mixr[:, cols_of(n)].astype(F32))
+                ).astype(BF16)
+
+            @pl.when(i > 0)
+            def _():
+                put_out(i - 1).start()
+
+            return 0
+
+        lax.fori_loop(0, 4, two, 0)
+        put_out(3).start()
         wait_for(xn.at[0], xsem.at[4])
         wait_for(mixs, xsem.at[6])
 
@@ -557,9 +573,13 @@
         def _():
             lax.fori_loop(0, 2, lambda half, _: (gu_conv(FFC - 1, half, pre_a), 0)[1], 0)
 
-        @pl.when((t == LAST - 2) | (t == LAST - 1))
-        def _():
-            down_first(4 * (t - LAST + 2))
+        @pl.when(t == LAST - 3)
+        def _():
+            down_part(0, 3)
+
+        @pl.when(t == LAST - 1)
+        def _():
+            down_part(3, 2)
 
         @pl.when(t == LAST)
         def _():
@@ -568,7 +588,19 @@
         return 0
 
     lax.fori_loop(0, LAST + 1, step, 0)
+    wait_for(out, osem)
     drain()
+
+
+def deliver(a, b, held, sems):
+    pieces = [pl.ds(i * 128, 128) for i in range(4)]
+    for i, r in enumerate(pieces):
+        pltpu.make_async_copy(a.at[r], held.at[r], sems.at[i]).start()
+    for i, r in enumerate(pieces):
+        pltpu.make_async_copy(a.at[r], held.at[r], sems.at[i]).wait()
+        pltpu.make_async_copy(held.at[r], b.at[r], sems.at[4 + i]).start()
+    for i, r in enumerate(pieces):
+        pltpu.make_async_copy(held.at[r], b.at[r], sems.at[4 + i]).wait()
 
 
 def angle_tables():
@@ -588,13 +620,14 @@
     vmem = pl.BlockSpec(memory_space=pltpu.VMEM)
     hbm = pl.BlockSpec(memory_space=pl.ANY)
     whole = jax.ShapeDtypeStruct((HALF, D), BF16)
-    return pl.pallas_call(
+    done = pl.pallas_call(
         layer,
         out_shape=whole,
         in_specs=[hbm] * 10 + [vmem] * 4,
-        out_specs=vmem,
+        out_specs=hbm,
         scratch_shapes=[
             pltpu.VMEM((C, 2, 4, 4, 64, COLS), BF16),
+            pltpu.VMEM((HALF, D), BF16),
             pltpu.VMEM((HALF, D), BF16),
             pltpu.VMEM((LENGTH, 128), F32),
             pltpu.VMEM((LENGTH, 128), F32),
@@ -616,6 +649,7 @@
             pltpu.SemaphoreType.DMA((8,)),
             pltpu.SemaphoreType.DMA((8,)),
             pltpu.SemaphoreType.DMA((8,)),
+            pltpu.SemaphoreType.DMA,
         ],
         compiler_params=pltpu.CompilerParams(
             collective_id=0, has_side_effects=True, vmem_limit_bytes=VLIM
@@ -624,6 +658,14 @@
         w_query, w_key, w_value, w_out.T, w_ffgate, w_ffup, w_down.T,
         tokens, jnp.asarray(cos), jnp.asarray(sin), mix_gain.reshape(1, D), ffn_gain.reshape(1, D), conv_gate, conv_up,
     )
+    return pl.pallas_call(
+        deliver,
+        out_shape=whole,
+        in_specs=[hbm],
+        out_specs=hbm,
+        scratch_shapes=[pltpu.VMEM((HALF, D), BF16), pltpu.SemaphoreType.DMA((8,))],
+        compiler_params=pltpu.CompilerParams(vmem_limit_bytes=67043328),
+    )(done)
 
 
 def solution(mesh):

time: 118 us -> 116 us (0.983)
  local copies, waits for them, and re-layouts: 3.16 us -> 0 us
    unnamed x1 -> x0, local copies, waits for them, and re-layouts: 3.16 us -> none
    pallas_call x0 -> x1, Pallas kernels: none -> 2.42 us  [body(): pl.pallas_call(deliver, out_shape=whole, in_specs=[hbm], out_specs=hbm, s...]
    pallas_call x1, Pallas kernels: 115 us -> 113 us  [body(): pl.pallas_call(layer, out_shape=whole, in_specs=[hbm] * 10 + [vmem] * 4,...]
where the time goes in v3:
time: 116 us
  Pallas kernels  116 us (100%)
    pallas_call x1, Pallas kernels, body(): pl.pallas_call(layer, out_shape=whole, in_specs=[hbm] * 10 + [vmem] * 4,...  113 us
    pallas_call x1, Pallas kernels, body(): pl.pallas_call(deliver, out_shape=whole, in_specs=[hbm], out_specs=hbm, s...  2.42 us

profile of v3, /device:TPU:1, one launch (start us, length us, event | category | flops | bytes accessed | tf_op | source)
XLA Modules:
  0.0 115.7 jit_solution(2313151706704100441)
XLA Ops:
  0.0 113.3 %shard_map.136.a = bf16[512,2048]{1,0:T(8,128)(2,1)} custom-call(bf16[64,256]{1,0:T(8,128)(2,1)} %w_query.1, bf16[64,256]{1,0:T(8,128)(2,1)} %w_key.1, bf16[64,512]{1,0:T(8,128)(2,1)} %w_value.1, bf16[64,512]{1,0:T(8,128)(2,1)} %bitcast.5, bf16[64,1408]{1,0:T(8,128)(2,1)} %w_ffgate.1, bf16[64,1408]{1,0:T(8,128)(2,1)} %w_ffup.1, bf16[64,1408]{1,0:T(8,128)(2,1)} %bitcast.4, ...), custom_call_target="tpu_custom_call" | custom-call | tf_op jit(solution)/shard_map/pallas_call | solution.py:623
  113.3 2.4 %shard_map.137 = bf16[512,2048]{1,0:T(8,128)(2,1)} custom-call(bf16[512,2048]{1,0:T(8,128)(2,1)} %shard_map.136.a), custom_call_target="tpu_custom_call" | custom-call | tf_op jit(solution)/shard_map/pallas_call | solution.py:661

commit v4 on v3

--- a/solution.py
+++ b/solution.py
@@ -163,7 +163,7 @@
                 wait_for(r, send_sem.at[4 + 3 * half + i])
 
     def tick(t):
-        for s in range(2, 6):
+        for s in (5, 4, 3, 2):
             c = t - LAG * (s - 2)
 
             @pl.when((c >= 0) & (c < NORM))

time: 116 us -> 116 us (level)
  no operation moved by 1% of the time
where the time goes in v4:
time: 116 us
  Pallas kernels  116 us (100%)
    pallas_call x1, Pallas kernels, body(): pl.pallas_call(layer, out_shape=whole, in_specs=[hbm] * 10 + [vmem] * 4,...  114 us
    pallas_call x1, Pallas kernels, body(): pl.pallas_call(deliver, out_shape=whole, in_specs=[hbm], out_specs=hbm, s...  2.42 us

profile of v4, /device:TPU:1, one launch (start us, length us, event | category | flops | bytes accessed | tf_op | source)
XLA Modules:
  0.0 116.2 jit_solution(4732942702961983929)
XLA Ops:
  0.0 113.8 %shard_map.136.a = bf16[512,2048]{1,0:T(8,128)(2,1)} custom-call(bf16[64,256]{1,0:T(8,128)(2,1)} %w_query.1, bf16[64,256]{1,0:T(8,128)(2,1)} %w_key.1, bf16[64,512]{1,0:T(8,128)(2,1)} %w_value.1, bf16[64,512]{1,0:T(8,128)(2,1)} %bitcast.5, bf16[64,1408]{1,0:T(8,128)(2,1)} %w_ffgate.1, bf16[64,1408]{1,0:T(8,128)(2,1)} %w_ffup.1, bf16[64,1408]{1,0:T(8,128)(2,1)} %bitcast.4, ...), custom_call_target="tpu_custom_call" | custom-call | tf_op jit(solution)/shard_map/pallas_call | solution.py:623
  113.8 2.4 %shard_map.137 = bf16[512,2048]{1,0:T(8,128)(2,1)} custom-call(bf16[512,2048]{1,0:T(8,128)(2,1)} %shard_map.136.a), custom_call_target="tpu_custom_call" | custom-call | tf_op jit(solution)/shard_map/pallas_call | solution.py:661
